TPU v7x, 32 devices: a whole 2x2x4 slice. The times are simulated.
32 devices in a mesh: sp: 4 (over z), tp: 4 (over y, x), dp: 2 (over core).
Axes of the slice: x: 2, y: 2, z: 4, core: 2. Of those that a mesh axis runs over, the one named last changes fastest.
Arguments:
- latent: bfloat16 [2, 1024, 2048], P('dp', ('sp', 'tp')), may hold values from -6 to 6
- condition: bfloat16 [2, 2048], P('dp', ('sp', 'tp')), may hold values from -6 to 6
- context: bfloat16 [2, 32, 2048], P('dp', 'sp'), may hold values from -6 to 6
- context_vector: bfloat16 [2048], P(('sp', 'tp')), may hold values from -6 to 6
- modulator: bfloat16 [2048, 6144], P(('sp', 'tp')), may hold values from -0.3125 to 0.3125
- norm_gain: float32 [2048], replicated, may hold values from 0.1 to 1.9
- query_weight: bfloat16 [2048, 512], P(None, 'tp'), may hold values from -4 to 4
- key_weight: bfloat16 [2048, 512], P(None, 'tp'), may hold values from -0.125 to 0.125
- value_weight: bfloat16 [2048, 512], P(None, 'tp'), may hold values from -0.125 to 0.125
- head_gain: float32 [128], replicated, may hold values from 0.1 to 1.9
- lambdas: float32 [4], P('tp'), may hold values from 0.3 to 0.8
- context_bias: float32 [4, 2], P('tp'), may hold values from 1.3 to 2.7
- out_weight: bfloat16 [512, 2048], P('tp'), may hold values from -0.25 to 0.25
Outputs:
- updated: bfloat16 [2, 1024, 2048], P('dp', ('sp', 'tp'))
All inputs are finite; a program needn't handle non-finite values.
Results may differ from a plain program's by a relative error of at most 0.024.
Values may be sent and summed in bfloat16 or wider, within the bound.
A program may use at most 64 MiB of HBM per device.

v0:
```python
import jax
import jax.numpy as jnp
from jax import lax
from jax.sharding import PartitionSpec as P

EPSILON = 1e-06
OUT_SCALE = 0.8
KEY_BLOCK = 2048
LOW_START = -1e30


def modulate(inputs, gain_vector, shift_vector, scale_vector):
    as_float = inputs.astype(jnp.float32)
    normed = as_float * lax.rsqrt(jnp.mean(as_float * as_float, axis=-1, keepdims=True) + EPSILON)
    return (normed * gain_vector * (1.0 + scale_vector) + shift_vector).astype(jnp.bfloat16)


def fold_block(running, queries, keys_in, values_in, key_flags, bias_table, score_scale):
    run_max, run_total, summed = running
    scores = (
        jnp.einsum("qhmd,khmd->hmqk", queries, keys_in, preferred_element_type=jnp.float32)
        * score_scale
    )
    if key_flags is not None:
        scores = scores + bias_table[:, :, None, None] * key_flags
    new_max = jnp.maximum(run_max, jnp.max(scores, axis=-1))
    shrink = jnp.exp(run_max - new_max)
    weights = jnp.exp(scores - new_max[..., None])
    run_total = run_total * shrink + jnp.sum(weights, axis=-1)
    summed = summed * shrink[..., None] + jnp.einsum(
        "hmqk,khe->hmqe",
        weights.astype(jnp.bfloat16),
        values_in,
        preferred_element_type=jnp.float32,
    )
    return (new_max, run_total, summed)


def fold_keys(running, queries, keys_in, values_in, key_flags, bias_table, score_scale):
    full_blocks = keys_in.shape[0] // KEY_BLOCK
    if full_blocks > 1:
        edge = full_blocks * KEY_BLOCK
        stacked = (
            keys_in[:edge].reshape((full_blocks, KEY_BLOCK) + keys_in.shape[1:]),
            values_in[:edge].reshape((full_blocks, KEY_BLOCK) + values_in.shape[1:]),
        )
        if key_flags is not None:
            stacked = stacked + (key_flags[:edge].reshape(full_blocks, KEY_BLOCK),)

        def fold_step(current, block_data):
            flag_part = None if key_flags is None else block_data[2]
            return (
                fold_block(
                    current,
                    queries,
                    block_data[0],
                    block_data[1],
                    flag_part,
                    bias_table,
                    score_scale,
                ),
                None,
            )

        running, ignored = lax.scan(fold_step, running, stacked)
        keys_in = keys_in[edge:]
        values_in = values_in[edge:]
        key_flags = None if key_flags is None else key_flags[edge:]
    if keys_in.shape[0] > 0:
        running = fold_block(
            running, queries, keys_in, values_in, key_flags, bias_table, score_scale
        )
    return running


def body(
    latent,
    condition,
    context,
    context_vector,
    modulator,
    norm_gain,
    query_weight,
    key_weight,
    value_weight,
    head_gain,
    lambdas,
    context_bias,
    out_weight,
):
    model_width = latent.shape[2]
    local_heads = lambdas.shape[0]
    query_width = query_weight.shape[1]
    head_size = query_width // (2 * local_heads)
    value_size = value_weight.shape[1] // local_heads
    score_scale = head_size ** (-0.5)
    activated = jax.nn.silu(
        jnp.concatenate([condition, context_vector[None, :]], axis=0).astype(jnp.float32)
    )
    partial_terms = jnp.dot(
        activated.astype(jnp.bfloat16), modulator, preferred_element_type=jnp.float32
    )
    modulations = lax.psum(partial_terms, ("sp", "tp"))
    hidden = modulate(
        latent[0],
        norm_gain,
        modulations[0, :model_width],
        modulations[0, model_width : 2 * model_width],
    )
    ctx_hidden = modulate(
        context[0],
        norm_gain,
        modulations[1, :model_width],
        modulations[1, model_width : 2 * model_width],
    )
    gate_vector = modulations[0, 2 * model_width :]
    incoming = lax.all_gather(hidden, "tp", axis=0, tiled=True)
    projected = jnp.concatenate(
        [
            jnp.dot(incoming, query_weight, preferred_element_type=jnp.float32),
            jnp.dot(incoming, key_weight, preferred_element_type=jnp.float32),
            jnp.dot(incoming, value_weight, preferred_element_type=jnp.float32),
        ],
        axis=1,
    ).astype(jnp.bfloat16)
    query_rows = projected.shape[0]
    queries = projected[:, :query_width].reshape(query_rows, local_heads, 2, head_size)
    own_keys = projected[:, query_width : 2 * query_width]
    own_values = projected[:, 2 * query_width :]
    gathered_context = lax.all_gather(ctx_hidden, "sp", axis=0, tiled=True)
    ctx_keys = jnp.dot(gathered_context, key_weight, preferred_element_type=jnp.float32).astype(
        jnp.bfloat16
    )
    ctx_values = jnp.dot(gathered_context, value_weight, preferred_element_type=jnp.float32).astype(
        jnp.bfloat16
    )
    start_carry = (
        jnp.full((local_heads, 2, query_rows), LOW_START, jnp.float32),
        jnp.zeros((local_heads, 2, query_rows), jnp.float32),
        jnp.zeros((local_heads, 2, query_rows, value_size), jnp.float32),
    )
    pieces = (own_keys, own_values)
    initial = fold_keys(
        start_carry,
        queries,
        ctx_keys.reshape(-1, local_heads, 2, head_size),
        ctx_values.reshape(-1, local_heads, value_size),
        jnp.ones((ctx_keys.shape[0],), jnp.float32),
        context_bias,
        score_scale,
    )
    incoming = (
        lax.all_gather(pieces[0], "sp", axis=0, tiled=True),
        lax.all_gather(pieces[1], "sp", axis=0, tiled=True),
    )
    run_max, run_total, summed = fold_keys(
        initial,
        queries,
        incoming[0].reshape(-1, local_heads, 2, head_size),
        incoming[1].reshape(-1, local_heads, value_size),
        None,
        context_bias,
        score_scale,
    )
    mixed = (
        summed[:, 0] / run_total[:, 0, :, None]
        - lambdas[:, None, None] * summed[:, 1] / run_total[:, 1, :, None]
    )
    normed = (
        mixed
        * lax.rsqrt(jnp.mean(mixed * mixed, axis=-1, keepdims=True) + EPSILON)
        * head_gain
        * OUT_SCALE
    )
    attended = (
        jnp.transpose(normed, (1, 0, 2))
        .reshape(query_rows, local_heads * value_size)
        .astype(jnp.bfloat16)
    )
    exchanged = lax.all_to_all(attended, "tp", split_axis=0, concat_axis=1, tiled=True)
    whole_weight = lax.all_gather(out_weight, "tp", axis=0, tiled=True)
    branch = jnp.dot(exchanged, whole_weight, preferred_element_type=jnp.float32)
    result = (latent[0].astype(jnp.float32) + gate_vector * branch).astype(jnp.bfloat16)
    return result[None]


def solution(mesh):
    placed = (
        P("dp", ("sp", "tp"), None),
        P("dp", ("sp", "tp")),
        P("dp", "sp", None),
        P(("sp", "tp")),
        P(("sp", "tp"), None),
        P(),
        P(None, "tp"),
        P(None, "tp"),
        P(None, "tp"),
        P(),
        P("tp"),
        P("tp", None),
        P("tp", None),
    )
    return jax.shard_map(
        body, mesh=mesh, in_specs=placed, out_specs=P("dp", ("sp", "tp"), None), check_vma=False
    )
```

profile of v0, /device:TPU:0, one launch (start us, length us, event | category | flops | bytes accessed | tf_op | source)
XLA Modules:
  0.0 170.0 jit_solution(7644564545617815921)
XLA Ops:
  6.6 1.4 copy-done
  8.0 1.0 fusion.43
  9.0 78.7 %psum.7 = f32[2,6144]{1,0:T(2,128)S(1)} all-reduce(f32[2,6144]{1,0:T(2,128)S(1)} %fusion.43), channel_id=1, replica_groups=mesh['sp'=4,'tp'=4,'dp'=2] {'sp','tp'}, use_global_device_ids=true, to_apply=%region_0.1 | all-reduce | flops 12288 | bytes 98304 | tf_op jit(solution)/shard_map/psum | solution.py:103
  87.6 0.6 slice_add_fusion.1
  88.3 1.1 fusion.14
  89.4 1.6 fusion.18
  91.0 0.7 all-gather.5.cloned.1.call-update
  92.0 13.4 %all_gather.16 = bf16[32,2048]{1,0:T(8,128)(2,1)S(1)} all-gather(bf16[8,2048]{1,0:T(8,128)(2,1)S(1)} %fusion.27), channel_id=1, replica_groups=mesh['sp'=4,'tp'=4,'dp'=2] {'sp'}, dimensions={0}, use_global_device_ids=true | all-gather | bytes 163840 | tf_op jit(solution)/shard_map/all_gather | solution.py:130
  105.4 0.2 convolution_convert_fusion.4
  106.3 7.2 %all-gather.3.cloned.1.call-done = bf16[256,2048]{1,0:T(8,128)(2,1)} async-done(((bf16[64,2048]{1,0:T(8,128)(2,1)}), bf16[256,2048]{1,0:T(8,128)(2,1)}) %all-gather.3.cloned.1.call-update) | async-done | bytes 1048592 | tf_op jit(solution)/shard_map/all_gather | solution.py:117
  113.5 1.9 %convolution_convert_fusion.1 = bf16[256,128]{1,0:T(8,128)(2,1)S(1)} fusion(bf16[256,2048]{1,0:T(8,128)(2,1)} %all-gather.3.cloned.1.call-done, bf16[2048,128]{1,0:T(8,128)(2,1)} %param.20), kind=kOutput, calls=%fused_computation.13 | convolution fusion | flops 134250496 | bytes 1638400 | tf_op jit(solution)/shard_map/dot_general | solution.py:121
  115.4 14.6 %all_gather.17 = bf16[1024,128]{1,0:T(8,128)(2,1)} all-gather(bf16[256,128]{1,0:T(8,128)(2,1)S(1)} %convolution_convert_fusion.1), channel_id=1, replica_groups=mesh['sp'=4,'tp'=4,'dp'=2] {'sp'}, dimensions={0}, use_global_device_ids=true | all-gather | bytes 327680 | tf_op jit(solution)/shard_map/all_gather | solution.py:153
  130.0 1.8 %copy.30 = bf16[1024,128]{0,1:T(8,128)(2,1)} copy(bf16[1024,128]{1,0:T(8,128)(2,1)} %all_gather.17) | data formatting | bytes 524288 | tf_op jit(solution)/shard_map/all_gather | solution.py:153
  131.8 0.4 convolution_convert_fusion
  132.2 14.5 %all_gather.18 = bf16[1024,128]{1,0:T(8,128)(2,1)S(1)} all-gather(bf16[256,128]{1,0:T(8,128)(2,1)S(1)} %convolution_convert_fusion), channel_id=1, replica_groups=mesh['sp'=4,'tp'=4,'dp'=2] {'sp'}, dimensions={0}, use_global_device_ids=true | all-gather | bytes 327680 | tf_op jit(solution)/shard_map/all_gather | solution.py:154
  146.7 0.5 convolution_convert_fusion.2
  147.3 0.6 multiply_reduce_fusion
  147.9 1.3 copy-done.1
  149.2 0.5 fusion.10
  149.7 0.4 fusion.7
  150.2 2.1 %fusion.3 = f32[2,256]{1,0:T(2,128)S(1)} fusion(f32[2,256,1024]{2,1,0:T(8,128)} %copy-done.1, f32[2,256]{1,0:T(2,128)S(1)} %get-tuple-element.15), kind=kLoop, calls=%fused_computation.6 | loop fusion | flops 1572352 | bytes 2101248 | tf_op jit(solution)/shard_map/reduce_sum | solution.py:29
  152.3 0.2 fusion.22
  153.0 7.4 %all_to_all.16 = bf16[4,64,128]{2,1,0:T(8,128)(2,1)S(1)} all-to-all(bf16[4,64,128]{2,1,0:T(8,128)(2,1)S(1)} %multiply_convert_fusion), channel_id=1, replica_groups=mesh['sp'=4,'tp'=4,'dp'=2] {'tp'}, dimensions={0} | all-to-all | bytes 131072 | tf_op jit(solution)/shard_map/all_to_all | solution.py:180
  160.4 2.8 %fusion.2 = bf16[1,64,2048]{2,1,0:T(8,128)(2,1)} fusion(bf16[512,2048]{1,0:T(8,128)(2,1)} %all-gather.5.cloned.1.call-done, bf16[1,64,2048]{2,1,0:T(8,128)(2,1)S(1)} %copy-done.3, f32[2048]{0:T(1024)S(1)} %bitcast.94, bf16[4,64,128]{2,1,0:T(8,128)(2,1)S(1)} %all_to_all.16), kind=kOutput, calls=%fused_computation.3 | convolution fusion | flops 134742016 | bytes 2695168 | tf_op jit(solution)/shard_map/dot_general | solution.py:182
  (44 shorter events, 1.1 us)
Async XLA Ops:
  6.5 1.4 copy-start
  6.5 82.8 %copy-start.3 = (bf16[1,64,2048]{2,1,0:T(8,128)(2,1)S(1)}, bf16[1,64,2048]{2,1,0:T(8,128)(2,1)}, u32[]{:S(2)}) copy-start(bf16[1,64,2048]{2,1,0:T(8,128)(2,1)} %param.13) | copy-start | bytes 786436
  6.5 85.4 %copy-start.10 = (f32[2048]{0:T(1024)S(1)}, f32[2048]{0:T(1024)}, u32[]{:S(2)}) copy-start(f32[2048]{0:T(1024)} %param.18) | copy-start | bytes 24580
  6.5 85.2 %copy-start.8 = (bf16[1,8,2048]{2,1,0:T(8,128)(2,1)S(1)}, bf16[1,8,2048]{2,1,0:T(8,128)(2,1)}, u32[]{:S(2)}) copy-start(bf16[1,8,2048]{2,1,0:T(8,128)(2,1)} %param.15) | copy-start | bytes 98308
  6.5 98.8 %copy-start.5 = (bf16[2048,128]{1,0:T(8,128)(2,1)S(1)}, bf16[2048,128]{1,0:T(8,128)(2,1)}, u32[]{:S(2)}) copy-start(bf16[2048,128]{1,0:T(8,128)(2,1)} %param.20) | copy-start | bytes 1572868
  6.6 107.0 %all-gather.3.cloned.1.call-start = ((), (), s32[]{:S(2)}) async-start(), calls=%async_computation.1 | async-start | bytes 1310720 | tf_op jit(solution)/shard_map/all_gather | solution.py:117
  91.0 40.8 %copy-start.4 = (bf16[2048,128]{1,0:T(8,128)(2,1)S(1)}, bf16[2048,128]{1,0:T(8,128)(2,1)}, u32[]{:S(2)}) copy-start(bf16[2048,128]{1,0:T(8,128)(2,1)} %param.21) | copy-start | bytes 1572868
  91.0 69.4 %all-gather.5.cloned.1.call-start = ((), (), s32[]{:S(2)}) async-start(), calls=%async_computation.2 | async-start | bytes 2621440 | tf_op jit(solution)/shard_map/all_gather | solution.py:181
  113.5 18.3 %copy-start.2 = (bf16[256,2048]{1,0:T(8,128)(2,1)S(1)}, bf16[256,2048]{1,0:T(8,128)(2,1)}, u32[]{:S(2)}) copy-start(bf16[256,2048]{1,0:T(8,128)(2,1)} %all-gather.3.cloned.1.call-done) | copy-start | bytes 3145732
  131.8 14.9 %copy-start.7 = (bf16[2048,128]{1,0:T(8,128)(2,1)S(1)}, bf16[2048,128]{1,0:T(8,128)(2,1)}, u32[]{:S(2)}) copy-start(bf16[2048,128]{1,0:T(8,128)(2,1)} %param.19) | copy-start | bytes 1572868
  131.8 15.4 %copy-start.11 = (f32[1,2]{1,0:T(1,128)S(1)}, f32[1,2]{1,0:T(1,128)}, u32[]{:S(2)}) copy-start(f32[1,2]{1,0:T(1,128)} %param.24) | copy-start | bytes 28
  131.8 15.6 %copy-start.6 = (bf16[1024,128]{0,1:T(8,128)(2,1)S(1)}, bf16[1024,128]{0,1:T(8,128)(2,1)}, u32[]{:S(2)}) copy-start(bf16[1024,128]{0,1:T(8,128)(2,1)} %copy.30) | copy-start | bytes 786436
  147.9 1.3 copy-start.1
  149.7 3.1 %copy-start.12 = (f32[128]{0:T(128)S(1)}, f32[128]{0:T(128)}, u32[]{:S(2)}) copy-start(f32[128]{0:T(128)} %param.22) | copy-start | bytes 1540
  149.7 10.6 %copy-start.9 = (f32[1,2048]{1,0:T(1,128)S(1)}, f32[1,2048]{1,0:T(1,128)}, u32[]{:S(2)}) copy-start(f32[1,2048]{1,0:T(1,128)} %get-tuple-element.13) | copy-start | bytes 24580
Sparse Core Ops, SparseCore 0:
  91.1 22.3 all-gather.2
  115.3 35.1 all-gather.4
where the time goes:
time: 170 us
  blocking collectives  129 us (76%)
  between operations  14.3 us (8%)
  matrix products  8.34 us (5%)
  waiting for transfers between devices  7.88 us (5%)
  other arithmetic  6.08 us (4%)
  local copies, waits for them, and re-layouts  4.84 us (3%)
    psum x1, blocking collectives, body(): modulations = lax.psum(partial_terms, ('sp', 'tp'))  78.7 us
    all_gather x1, blocking collectives, body(): lax.all_gather(pieces[0], 'sp', axis=0, tiled=True)  14.6 us
    all_gather x1, blocking collectives, body(): lax.all_gather(pieces[1], 'sp', axis=0, tiled=True)  14.5 us
    all_gather x1, blocking collectives, body(): gathered_context = lax.all_gather(ctx_hidden, 'sp', axis=0, tiled=True)  13.4 us
    all_to_all x1, blocking collectives, body(): lax.all_to_all(attended, 'tp', split_axis=0, concat_axis=1, tiled=True)  7.38 us
    all_gather x1, waiting for transfers between devices, body(): incoming = lax.all_gather(hidden, 'tp', axis=0, tiled=True)  7.17 us
  transfers between devices with their start and end apart: 2, of which 1 were waited for; matrix products, arithmetic and copies ran while one was open for 6% of the time, Pallas kernels for 0%

commit v1 on v0

--- a/solution.py
+++ b/solution.py
@@ -1,6 +1,10 @@
+import functools
+
 import jax
 import jax.numpy as jnp
 from jax import lax
+from jax.experimental import pallas as pl
+from jax.experimental.pallas import tpu as pltpu
 from jax.sharding import PartitionSpec as P
 
 EPSILON = 1e-06
@@ -184,6 +188,450 @@
     return result[None]
 
 
+MESH = pl.DeviceIdType.MESH
+LANES = 128
+
+
+def fused_kernel(
+    sp_n, tp_n, score_scale,
+    latent, condition, context, context_vector, modulator, norm_gain,
+    query_weight, key_weight, value_weight, head_gain, lambdas, context_bias, out_weight,
+    out,
+    mod_v, part, rs_in, mods, lat, ctx_all, w_q, w_kv, w_out, vecs, hid, kvb, att_out, att_in,
+    own_sem, rs_ss, rs_rs, ag_ss, ag_rs, lat_ss, lat_rs, ctx_ss, ctx_rs,
+    kv_os, kv_ss, kv_rs, wt_ss, wt_rs, wd_ss, wd_rs, at_ss, at_rs,
+):
+    sp = lax.axis_index("sp")
+    tp = lax.axis_index("tp")
+    dp = lax.axis_index("dp")
+    n = sp_n * tp_n
+    rank = sp * tp_n + tp
+    half = lat.shape[1]
+    width = lat.shape[2]
+    rows = half * 2
+    qrows = rows * tp_n
+    chunk = part.shape[2]
+
+    barrier = pltpu.get_barrier_semaphore()
+
+    def greet(d, carry):
+        peer = lax.rem(rank + d, n)
+        pl.semaphore_signal(
+            barrier, inc=1, device_id=(peer // tp_n, lax.rem(peer, tp_n), dp), device_id_type=MESH
+        )
+        return carry
+
+    lax.fori_loop(1, n, greet, 0)
+    pl.semaphore_signal(barrier, inc=1, device_id=(sp, tp, 1 - dp), device_id_type=MESH)
+
+    loads = [
+        pltpu.make_async_copy(modulator, mod_v, own_sem.at[0]),
+        pltpu.make_async_copy(latent, lat.at[pl.ds(tp * 2, 2)], own_sem.at[1]),
+        pltpu.make_async_copy(key_weight, w_kv.at[:, pl.ds(0, LANES)], own_sem.at[2]),
+        pltpu.make_async_copy(value_weight, w_kv.at[:, pl.ds(LANES, LANES)], own_sem.at[3]),
+        pltpu.make_async_copy(query_weight, w_q, own_sem.at[4]),
+        pltpu.make_async_copy(out_weight, w_out.at[pl.ds(tp * 4, 4)], own_sem.at[5]),
+    ]
+    for load in loads:
+        load.start()
+
+    rows_in = jnp.concatenate([condition[...], context_vector[...]], axis=0).astype(jnp.float32)
+    activated = jax.nn.silu(rows_in).astype(jnp.bfloat16)
+    loads[0].wait()
+    partial_terms = jnp.dot(activated, mod_v[...], preferred_element_type=jnp.float32)
+    for p in range(n):
+        part[p] = partial_terms[:, p * chunk : (p + 1) * chunk]
+    loads[1].wait()
+    pl.semaphore_wait(barrier, n)
+
+    def rs_copy(d):
+        peer = lax.rem(rank + d, n)
+        return pltpu.make_async_remote_copy(
+            src_ref=part.at[peer], dst_ref=rs_in.at[d], send_sem=rs_ss.at[d], recv_sem=rs_rs.at[d],
+            device_id=(peer // tp_n, lax.rem(peer, tp_n), dp), device_id_type=MESH,
+        )
+
+    def ag_copy(d):
+        peer = lax.rem(rank + d, n)
+        return pltpu.make_async_remote_copy(
+            src_ref=mods.at[rank], dst_ref=mods.at[rank], send_sem=ag_ss.at[d], recv_sem=ag_rs.at[d],
+            device_id=(peer // tp_n, lax.rem(peer, tp_n), dp), device_id_type=MESH,
+        )
+
+    def ag_arrival(d):
+        peer = lax.rem(rank - d + n, n)
+        return pltpu.make_async_remote_copy(
+            src_ref=mods.at[peer], dst_ref=mods.at[peer], send_sem=ag_ss.at[d], recv_sem=ag_rs.at[d],
+            device_id=(peer // tp_n, lax.rem(peer, tp_n), dp), device_id_type=MESH,
+        )
+
+    def each(first, last, act):
+        def step(d, carry):
+            act(d)
+            return carry
+
+        lax.fori_loop(first, last, step, 0)
+
+    each(1, n, lambda d: rs_copy(d).start())
+
+    across = tp + 1 - 2 * lax.rem(tp, 2)
+    along = lax.rem(tp + 2, 4)
+    corner = along + 1 - 2 * lax.rem(along, 2)
+
+    class Plane:
+        def __init__(self, buf, index, ss, rs):
+            self.buf, self.index, self.ss, self.rs = buf, index, ss, rs
+
+        def copy(self, owner, part_no, target, slot, kind):
+            place = self.buf.at[self.index(owner, part_no)]
+            return pltpu.make_async_remote_copy(
+                src_ref=place, dst_ref=place, send_sem=self.ss.at[slot],
+                recv_sem=self.rs.at[kind * 2 + part_no],
+                device_id=(sp, target, dp), device_id_type=MESH,
+            )
+
+        def first(self):
+            return [
+                self.copy(tp, 0, across, 0, 0),
+                self.copy(tp, 1, along, 1, 1),
+                self.copy(tp, 1, across, 2, 0),
+                self.copy(tp, 0, along, 3, 1),
+            ]
+
+        def relays(self):
+            return [self.copy(across, 0, along, 4, 2), self.copy(along, 1, across, 5, 2)]
+
+        def arrival(self, kind, part_no):
+            owner = (across, along, corner)[kind]
+            return self.copy(owner, part_no, across, 0, kind)
+
+    plane = Plane(lat, lambda o, q: o * 2 + q, lat_ss, lat_rs)
+    lat_first = plane.first()
+    for copy in lat_first:
+        copy.start()
+
+    def ctx_copy(d):
+        peer = lax.rem(sp + d, sp_n)
+        return pltpu.make_async_remote_copy(
+            src_ref=context, dst_ref=ctx_all.at[sp], send_sem=ctx_ss.at[d], recv_sem=ctx_rs.at[d],
+            device_id=(peer, tp, dp), device_id_type=MESH,
+        )
+
+    def ctx_arrival(d):
+        peer = lax.rem(sp - d + sp_n, sp_n)
+        return pltpu.make_async_remote_copy(
+            src_ref=context, dst_ref=ctx_all.at[peer], send_sem=ctx_ss.at[d], recv_sem=ctx_rs.at[d],
+            device_id=(peer, tp, dp), device_id_type=MESH,
+        )
+
+    for d in range(1, sp_n):
+        ctx_copy(d).start()
+    ctx_all[sp] = context[...]
+    rs_in[0] = part[rank]
+
+    each(1, n, lambda d: rs_copy(d).wait_recv())
+    total = rs_in[0]
+    for d in range(1, n):
+        total = total + rs_in[d]
+    mods[rank] = total
+    each(1, n, lambda d: ag_copy(d).start())
+
+    lat_relays = plane.relays()
+    plane.arrival(0, 0).wait_recv()
+    lat_relays[0].start()
+    plane.arrival(1, 1).wait_recv()
+    lat_relays[1].start()
+
+    for d in range(1, sp_n):
+        ctx_arrival(d).wait_recv()
+    each(1, n, lambda d: ag_arrival(d).wait_recv())
+    whole = jnp.concatenate([mods[p] for p in range(n)], axis=1)
+    gain = norm_gain[...]
+    vecs[0:1, :] = gain * (1.0 + whole[0:1, width : 2 * width])
+    vecs[1:2, :] = whole[0:1, :width]
+    vecs[2:3, :] = gain * (1.0 + whole[1:2, width : 2 * width])
+    vecs[3:4, :] = whole[1:2, :width]
+    vecs[4:5, :] = whole[0:1, 2 * width :]
+
+    def normed_rows(x, at):
+        x = x.astype(jnp.float32)
+        scale = lax.rsqrt(jnp.mean(x * x, axis=-1, keepdims=True) + EPSILON)
+        return (x * scale * vecs[at : at + 1, :] + vecs[at + 1 : at + 2, :]).astype(jnp.bfloat16)
+
+    def norm_block(owner):
+        for q in range(2):
+            at = pl.multiple_of((owner * 2 + q) * half, half)
+            hid[pl.ds(at, half), :] = normed_rows(lat[owner * 2 + q], 0)
+
+    ctx_rows = ctx_all.shape[0] * ctx_all.shape[1]
+    hid[qrows : qrows + ctx_rows, :] = normed_rows(
+        ctx_all[...].astype(jnp.float32).reshape(ctx_rows, width), 2
+    )
+    norm_block(tp)
+    plane.arrival(0, 1).wait_recv()
+    norm_block(across)
+    plane.arrival(1, 0).wait_recv()
+    norm_block(along)
+    plane.arrival(2, 0).wait_recv()
+    plane.arrival(2, 1).wait_recv()
+    norm_block(corner)
+
+    for load in loads[2:]:
+        load.wait()
+    kv = jnp.dot(hid[...], w_kv[...], preferred_element_type=jnp.float32).astype(jnp.bfloat16)
+    kvb[sp] = kv[:qrows]
+    ctx_kv = kv[qrows:]
+
+    def kv_own(to, slot):
+        return pltpu.make_async_remote_copy(
+            src_ref=kvb.at[sp], dst_ref=kvb.at[sp], send_sem=kv_os.at[slot], recv_sem=kv_rs.at[sp],
+            device_id=(to, tp, dp), device_id_type=MESH,
+        )
+
+    @pl.when(sp + 1 < sp_n)
+    def _():
+        kv_own(sp + 1, 0).start()
+
+    @pl.when(sp > 0)
+    def _():
+        kv_own(sp - 1, 1).start()
+
+    wplane = Plane(w_out, lambda o, q: o * 4 + dp * 2 + q, wt_ss, wt_rs)
+    w_first = wplane.first()
+    for copy in w_first:
+        copy.start()
+
+    queries = jnp.dot(hid[:qrows, :], w_q[...], preferred_element_type=jnp.float32) * score_scale
+    queries = queries.astype(jnp.bfloat16)
+    head = queries.shape[1] // 2
+    lane = lax.broadcasted_iota(jnp.int32, queries.shape, 1)
+    zero = jnp.zeros_like(queries)
+    both = jnp.concatenate(
+        [jnp.where(lane < head, queries, zero), jnp.where(lane < head, zero, queries)], axis=0
+    )
+
+    def score(keys):
+        return lax.dot_general(
+            both, keys, (((1,), (1,)), ((), ())), preferred_element_type=jnp.float32
+        )
+
+    map_row = lax.broadcasted_iota(jnp.int32, (2 * qrows, 1), 0)
+    bias = jnp.where(map_row < qrows, context_bias[0, 0], context_bias[0, 1])
+
+    def fold(running, scores, values):
+        top = jnp.max(scores, axis=-1, keepdims=True)
+        if running is not None:
+            top = jnp.maximum(running[0], top)
+        weights = jnp.exp(scores - top)
+        count = jnp.sum(weights, axis=-1, keepdims=True)
+        summed = jnp.dot(weights.astype(jnp.bfloat16), values, preferred_element_type=jnp.float32)
+        if running is not None:
+            shrink = jnp.exp(running[0] - top)
+            count = running[1] * shrink + count
+            summed = running[2] * shrink + summed
+        return top, count, summed
+
+    running = fold(None, score(ctx_kv[:, :LANES]) + bias, ctx_kv[:, LANES:])
+    running = fold(running, score(kv[:qrows, :LANES]), kv[:qrows, LANES:])
+
+    w_relays = wplane.relays()
+    wplane.arrival(0, 0).wait_recv()
+    w_relays[0].start()
+    wplane.arrival(1, 1).wait_recv()
+    w_relays[1].start()
+
+    high = (2 * sp) // sp_n
+
+    def block_at(t):
+        up = (t - 1) + jnp.where(t - 1 >= sp, 1, 0)
+        down = (sp_n - t) - jnp.where(sp_n - t <= sp, 1, 0)
+        return jnp.where(high == 0, up, down)
+
+    def onward(b):
+        step = jnp.where(b < sp, 1, -1)
+        to = sp + step
+        ok = jnp.logical_and(to >= 0, to < sp_n)
+        safe = jnp.where(ok, to, sp - step)
+        return ok, pltpu.make_async_remote_copy(
+            src_ref=kvb.at[b], dst_ref=kvb.at[b], send_sem=kv_ss.at[b], recv_sem=kv_rs.at[b],
+            device_id=(safe, tp, dp), device_id_type=MESH,
+        )
+
+    def sibling(owner, part_no, slot):
+        place = w_out.at[owner * 4 + dp * 2 + part_no]
+        return pltpu.make_async_remote_copy(
+            src_ref=place, dst_ref=place, send_sem=wd_ss.at[slot], recv_sem=wd_rs.at[slot],
+            device_id=(sp, tp, 1 - dp), device_id_type=MESH,
+        )
+
+    def sibling_arrival(owner, part_no, slot):
+        place = w_out.at[owner * 4 + (1 - dp) * 2 + part_no]
+        return pltpu.make_async_remote_copy(
+            src_ref=place, dst_ref=place, send_sem=wd_ss.at[slot], recv_sem=wd_rs.at[slot],
+            device_id=(sp, tp, 1 - dp), device_id_type=MESH,
+        )
+
+    owners = (across, along, corner)
+    sent = []
+    for t in range(1, sp_n):
+        b = block_at(t)
+        ok, copy = onward(b)
+        copy.wait_recv()
+        pl.when(ok)(copy.start)
+        sent.append((ok, copy))
+        running = fold(running, score(kvb[b, :, :LANES]), kvb[b, :, LANES:])
+
+    top, count, summed = running
+    shares = summed / count
+    mixed = shares[:qrows] - lambdas[0] * shares[qrows:]
+    normed = (
+        mixed
+        * lax.rsqrt(jnp.mean(mixed * mixed, axis=-1, keepdims=True) + EPSILON)
+        * head_gain[...]
+        * OUT_SCALE
+    ).astype(jnp.bfloat16)
+    for p in range(tp_n):
+        att_out[p] = normed[p * rows : (p + 1) * rows]
+
+    def at_copy(d):
+        peer = lax.rem(tp + d, tp_n)
+        return pltpu.make_async_remote_copy(
+            src_ref=att_out.at[peer], dst_ref=att_in.at[tp], send_sem=at_ss.at[d], recv_sem=at_rs.at[d],
+            device_id=(sp, peer, dp), device_id_type=MESH,
+        )
+
+    def at_arrival(d):
+        peer = lax.rem(tp - d + tp_n, tp_n)
+        return pltpu.make_async_remote_copy(
+            src_ref=att_out.at[peer], dst_ref=att_in.at[peer], send_sem=at_ss.at[d], recv_sem=at_rs.at[d],
+            device_id=(sp, peer, dp), device_id_type=MESH,
+        )
+
+    for d in range(1, tp_n):
+        at_copy(d).start()
+    att_in[tp] = att_out[tp]
+
+    w_sent = []
+    for kind, part_no in ((0, 0), (1, 1), (0, 1), (1, 0), (2, 0), (2, 1)):
+        if (kind, part_no) not in ((0, 0), (1, 1)):
+            wplane.arrival(kind, part_no).wait_recv()
+        copy = sibling(owners[kind], part_no, kind * 2 + part_no)
+        copy.start()
+        w_sent.append(copy)
+    for kind in range(3):
+        for part_no in range(2):
+            sibling_arrival(owners[kind], part_no, kind * 2 + part_no).wait_recv()
+    for d in range(1, tp_n):
+        at_arrival(d).wait_recv()
+
+    attended = jnp.concatenate([att_in[p] for p in range(tp_n)], axis=1)
+    step = 512
+    for first in range(0, width, step):
+        cols = slice(first, first + step)
+        weight = w_out[:, :, cols].reshape(attended.shape[1], step)
+        branch = jnp.dot(attended, weight, preferred_element_type=jnp.float32)
+        for q in range(2):
+            mine = lat[tp * 2 + q, :, cols].astype(jnp.float32)
+            update = mine + vecs[4:5, cols] * branch[q * half : (q + 1) * half]
+            out[q * half : (q + 1) * half, cols] = update.astype(jnp.bfloat16)
+
+    each(1, n, lambda d: rs_copy(d).wait_send())
+    each(1, n, lambda d: ag_copy(d).wait_send())
+    for copy in lat_first + lat_relays + w_first + w_relays + w_sent:
+        copy.wait_send()
+    for d in range(1, sp_n):
+        ctx_copy(d).wait_send()
+    pl.when(sp + 1 < sp_n)(lambda: kv_own(sp + 1, 0).wait_send())
+    pl.when(sp > 0)(lambda: kv_own(sp - 1, 1).wait_send())
+    for ok, copy in sent:
+        pl.when(ok)(copy.wait_send)
+    for d in range(1, tp_n):
+        at_copy(d).wait_send()
+
+
+def fused(
+    axes, latent, condition, context, context_vector, modulator, norm_gain, query_weight,
+    key_weight, value_weight, head_gain, lambdas, context_bias, out_weight,
+):
+    sp_n, tp_n, dp_n = axes
+    n = sp_n * tp_n
+    rows, width = latent.shape[1:]
+    half = rows // 2
+    chunk = modulator.shape[1] // n
+    ctx_rows = context.shape[1]
+    qw = query_weight.shape[1]
+    value = value_weight.shape[1]
+    qrows = rows * tp_n
+    wrows = out_weight.shape[0] // 4
+    bf, f32 = jnp.bfloat16, jnp.float32
+    vm = pl.BlockSpec(memory_space=pltpu.VMEM)
+    sm = pl.BlockSpec(memory_space=pltpu.SMEM)
+    hb = pl.BlockSpec(memory_space=pl.ANY)
+    dma = lambda k: pltpu.SemaphoreType.DMA((k,))
+    result = pl.pallas_call(
+        functools.partial(fused_kernel, sp_n, tp_n, (qw // 2) ** (-0.5)),
+        out_shape=jax.ShapeDtypeStruct((rows, width), bf),
+        in_specs=[hb, vm, vm, vm, hb, vm, hb, hb, hb, vm, sm, sm, hb],
+        out_specs=vm,
+        scratch_shapes=[
+            pltpu.VMEM(modulator.shape, bf),
+            pltpu.VMEM((n, 2, chunk), f32),
+            pltpu.VMEM((n, 2, chunk), f32),
+            pltpu.VMEM((n, 2, chunk), f32),
+            pltpu.VMEM((tp_n * 2, half, width), bf),
+            pltpu.VMEM((sp_n, ctx_rows, width), bf),
+            pltpu.VMEM((width, qw), bf),
+            pltpu.VMEM((width, qw + value), bf),
+            pltpu.VMEM((tp_n * 4, wrows, width), bf),
+            pltpu.VMEM((8, width), f32),
+            pltpu.VMEM((qrows + sp_n * ctx_rows, width), bf),
+            pltpu.VMEM((sp_n, qrows, qw + value), bf),
+            pltpu.VMEM((tp_n, rows, value), bf),
+            pltpu.VMEM((tp_n, rows, value), bf),
+            dma(6), dma(n), dma(n), dma(n), dma(n), dma(6), dma(6), dma(sp_n), dma(sp_n),
+            dma(2), dma(sp_n), dma(sp_n), dma(6), dma(6), dma(6), dma(6), dma(tp_n), dma(tp_n),
+        ],
+        compiler_params=pltpu.CompilerParams(
+            collective_id=0, has_side_effects=True, vmem_limit_bytes=48 * 2**20
+        ),
+        name="fused_block",
+    )(
+        latent.reshape(2, half, width),
+        condition,
+        context[0],
+        context_vector[None, :],
+        modulator,
+        norm_gain[None, :],
+        query_weight,
+        key_weight,
+        value_weight,
+        head_gain[None, :],
+        lambdas,
+        context_bias,
+        out_weight.reshape(4, wrows, width),
+    )
+    return result[None]
+
+
+def choose(axes, *arrays):
+    sp_n, tp_n, dp_n = axes
+    latent, modulator, query_weight, value_weight = arrays[0], arrays[4], arrays[6], arrays[8]
+    lambdas, out_weight = arrays[10], arrays[12]
+    fits = (
+        tp_n == 4
+        and dp_n == 2
+        and 1 < sp_n <= 8
+        and lambdas.shape[0] == 1
+        and query_weight.shape[1] == LANES
+        and value_weight.shape[1] == LANES
+        and modulator.shape[1] % (sp_n * tp_n * LANES) == 0
+        and latent.shape[1] % 32 == 0
+        and latent.shape[2] % 512 == 0
+        and out_weight.shape[0] % 64 == 0
+    )
+    return fused(axes, *arrays) if fits else body(*arrays)
+
+
 def solution(mesh):
     placed = (
         P("dp", ("sp", "tp"), None),
@@ -200,6 +648,7 @@
         P("tp", None),
         P("tp", None),
     )
+    axes = (mesh.shape["sp"], mesh.shape["tp"], mesh.shape["dp"])
     return jax.shard_map(
-        body, mesh=mesh, in_specs=placed, out_specs=P("dp", ("sp", "tp"), None), check_vma=False
-    )
+        functools.partial(choose, axes), mesh=mesh, in_specs=placed, out_specs=P("dp", ("sp", "tp"), None), check_vma=False
+    )

time: 170 us -> 50 us (0.29)
  blocking collectives: 129 us -> 0 us
  Pallas kernels: 0 us -> 37.5 us
  between operations: 14.3 us -> 0.68 us
  matrix products: 8.34 us -> 0 us
  waiting for transfers between devices: 7.88 us -> 0 us
  local copies, waits for them, and re-layouts: 4.84 us -> 11.3 us
  other arithmetic: 6.08 us -> 0 us
    psum x1 -> x0, blocking collectives: 78.7 us -> none  [body(): modulations = lax.psum(partial_terms, ('sp', 'tp'))]
    all_gather x3 -> x0, blocking collectives: 42.5 us -> none  [the longest x1 14.6 us: body(): lax.all_gather(pieces[0], 'sp', axis=0, tiled=True)]
    pallas_call x0 -> x1, Pallas kernels: none -> 37.5 us  [fused(): pl.pallas_call(functools.partial(fused_kernel, sp_n, tp_n, (qw // 2) ** (...]
    unnamed x26 -> x25, local copies, waits for them, and re-layouts: 2.69 us -> 11.3 us
    dot_general x10 -> x0, matrix products: 8.34 us -> none  [the longest x1 2.78 us: body(): jnp.dot(exchanged, whole_weight, preferred_element_type=jnp.float32)]
    all_to_all x1 -> x0, blocking collectives: 7.38 us -> none  [body(): lax.all_to_all(attended, 'tp', split_axis=0, concat_axis=1, tiled=True)]
    all_gather x2 -> x0, waiting for transfers between devices: 7.17 us -> none  [the longest x1 7.17 us: body(): incoming = lax.all_gather(hidden, 'tp', axis=0, tiled=True)]
    reduce_sum x5 -> x0, other arithmetic: 3.56 us -> none  [the longest x2 2.11 us: fold_block(): run_total = run_total * shrink + jnp.sum(weights, axis=-1)]
  transfers between devices with their start and end apart: 2 -> 0, of which waited for: 1 -> 0; matrix products, arithmetic and copies ran while one was open for 6% -> 0% of each run, Pallas kernels for 0% -> 0%
where the time goes in v1:
time: 50 us; the launch traced here: 49.5 us
  Pallas kernels  37.5 us (75%)
  local copies, waits for them, and re-layouts  11.3 us (23%)
  between operations  0.68 us (1%)
    pallas_call x1, Pallas kernels, fused(): pl.pallas_call(functools.partial(fused_kernel, sp_n, tp_n, (qw // 2) ** (...  37.5 us
    unnamed x25, local copies, waits for them, and re-layouts  11.3 us

profile of v1, /device:TPU:0, one launch (start us, length us, event | category | flops | bytes accessed | tf_op | source)
XLA Modules:
  0.0 49.5 jit_solution(16990294173740846802)
XLA Ops:
  0.7 0.0 copy-start
  0.7 1.4 %copy-done = bf16[128,6144]{1,0:T(8,128)(2,1)S(1)} copy-done((bf16[128,6144]{1,0:T(8,128)(2,1)S(1)}, bf16[128,6144]{1,0:T(8,128)(2,1)}, u32[]{:S(2)}) %copy-start) | copy-done | bytes 1572888
  2.1 0.0 copy-start.1
  2.1 1.0 %copy-done.1 = bf16[2048,128]{1,0:T(8,128)(2,1)S(1)} copy-done((bf16[2048,128]{1,0:T(8,128)(2,1)S(1)}, bf16[2048,128]{1,0:T(8,128)(2,1)}, u32[]{:S(2)}) %copy-start.1) | copy-done | bytes 524312
  3.1 0.0 copy-start.2
  3.1 1.0 %copy-done.2 = bf16[2048,128]{1,0:T(8,128)(2,1)S(1)} copy-done((bf16[2048,128]{1,0:T(8,128)(2,1)S(1)}, bf16[2048,128]{1,0:T(8,128)(2,1)}, u32[]{:S(2)}) %copy-start.2) | copy-done | bytes 524312
  4.1 0.0 copy-start.3
  4.1 1.0 %copy-done.3 = bf16[2048,128]{1,0:T(8,128)(2,1)S(1)} copy-done((bf16[2048,128]{1,0:T(8,128)(2,1)S(1)}, bf16[2048,128]{1,0:T(8,128)(2,1)}, u32[]{:S(2)}) %copy-start.3) | copy-done | bytes 524312
  5.2 0.0 copy-start.4
  5.2 1.0 %copy-done.4 = bf16[128,2048]{1,0:T(8,128)(2,1)S(1)} copy-done((bf16[128,2048]{1,0:T(8,128)(2,1)S(1)}, bf16[128,2048]{1,0:T(8,128)(2,1)}, u32[]{:S(2)}) %copy-start.4) | copy-done | bytes 524312
  6.2 0.0 copy-start.5
  6.2 0.9 %copy-done.5 = bf16[1,64,2048]{2,1,0:T(8,128)(2,1)S(1)} copy-done((bf16[1,64,2048]{2,1,0:T(8,128)(2,1)S(1)}, bf16[1,64,2048]{2,1,0:T(8,128)(2,1)}, u32[]{:S(2)}) %copy-start.5) | copy-done | bytes 262168
  7.2 0.0 copy-start.6
  7.2 0.8 %copy-done.6 = bf16[1,8,2048]{2,1,0:T(8,128)(2,1)S(1)} copy-done((bf16[1,8,2048]{2,1,0:T(8,128)(2,1)S(1)}, bf16[1,8,2048]{2,1,0:T(8,128)(2,1)}, u32[]{:S(2)}) %copy-start.6) | copy-done | bytes 32792
  7.9 0.0 copy-start.7
  7.9 0.7 %copy-done.7 = f32[2048]{0:T(1024)S(1)} copy-done((f32[2048]{0:T(1024)S(1)}, f32[2048]{0:T(1024)}, u32[]{:S(2)}) %copy-start.7) | copy-done | bytes 8216
  8.6 0.0 copy-start.8
  8.6 0.7 %copy-done.8 = bf16[1,128]{1,0:T(2,128)(2,1)S(1)} copy-done((bf16[1,128]{1,0:T(2,128)(2,1)S(1)}, bf16[1,128]{1,0:T(2,128)(2,1)}, u32[]{:S(2)}) %copy-start.8) | copy-done | bytes 280
  9.3 0.0 copy-start.9
  9.3 0.7 %copy-done.9 = bf16[128]{0:T(256)(128)(2,1)S(1)} copy-done((bf16[128]{0:T(256)(128)(2,1)S(1)}, bf16[128]{0:T(256)(128)(2,1)}, u32[]{:S(2)}) %copy-start.9) | copy-done | bytes 280
  9.9 0.7 %copy-done.10 = f32[128]{0:T(128)S(1)} copy-done((f32[128]{0:T(128)S(1)}, f32[128]{0:T(128)}, u32[]{:S(2)}) %copy-start.10) | copy-done | bytes 536
  10.6 0.7 %copy-done.11 = f32[1,2]{1,0:T(1,128)S(1)} copy-done((f32[1,2]{1,0:T(1,128)S(1)}, f32[1,2]{1,0:T(1,128)}, u32[]{:S(2)}) %copy-start.11) | copy-done | bytes 32
  11.3 37.5 %fused_block.1 = bf16[64,2048]{1,0:T(8,128)(2,1)S(1)} custom-call(bf16[2,32,2048]{2,1,0:T(8,128)(2,1)S(1)} %bitcast.9, bf16[1,128]{1,0:T(2,128)(2,1)S(1)} %copy-done.8, bf16[8,2048]{1,0:T(8,128)(2,1)S(1)} %bitcast.10, bf16[1,128]{1,0:T(2,128)(2,1)S(1)} %bitcast.12, bf16[128,6144]{1,0:T(8,128)(2,1)S(1)} %copy-done, f32[1,2048]{1,0:T(1,128)S(1)} %bitcast.11, ...), custom_call_target="tpu_custom_call" | custom-call | tf_op jit(solution)/shard_map/fused_block/pallas_call | solution.py:571
  48.8 0.7 %copy.16 = bf16[1,64,2048]{2,1,0:T(8,128)(2,1)} copy(bf16[1,64,2048]{2,1,0:T(8,128)(2,1)S(1)} %bitcast.7) | data formatting | bytes 524288
  (2 shorter events, 0.0 us)
Async XLA Ops:
  0.7 1.4 %copy-start = (bf16[128,6144]{1,0:T(8,128)(2,1)S(1)}, bf16[128,6144]{1,0:T(8,128)(2,1)}, u32[]{:S(2)}) copy-start(bf16[128,6144]{1,0:T(8,128)(2,1)} %modulator.1) | copy-start | bytes 4718596
  2.1 1.0 %copy-start.1 = (bf16[2048,128]{1,0:T(8,128)(2,1)S(1)}, bf16[2048,128]{1,0:T(8,128)(2,1)}, u32[]{:S(2)}) copy-start(bf16[2048,128]{1,0:T(8,128)(2,1)} %query_weight.1) | copy-start | bytes 1572868
  3.1 1.0 %copy-start.2 = (bf16[2048,128]{1,0:T(8,128)(2,1)S(1)}, bf16[2048,128]{1,0:T(8,128)(2,1)}, u32[]{:S(2)}) copy-start(bf16[2048,128]{1,0:T(8,128)(2,1)} %key_weight.1) | copy-start | bytes 1572868
  4.1 1.0 %copy-start.3 = (bf16[2048,128]{1,0:T(8,128)(2,1)S(1)}, bf16[2048,128]{1,0:T(8,128)(2,1)}, u32[]{:S(2)}) copy-start(bf16[2048,128]{1,0:T(8,128)(2,1)} %value_weight.1) | copy-start | bytes 1572868
  5.2 1.0 %copy-start.4 = (bf16[128,2048]{1,0:T(8,128)(2,1)S(1)}, bf16[128,2048]{1,0:T(8,128)(2,1)}, u32[]{:S(2)}) copy-start(bf16[128,2048]{1,0:T(8,128)(2,1)} %param.25) | copy-start | bytes 1572868
  6.2 0.9 %copy-start.5 = (bf16[1,64,2048]{2,1,0:T(8,128)(2,1)S(1)}, bf16[1,64,2048]{2,1,0:T(8,128)(2,1)}, u32[]{:S(2)}) copy-start(bf16[1,64,2048]{2,1,0:T(8,128)(2,1)} %param.13) | copy-start | bytes 786436
  7.2 0.8 %copy-start.6 = (bf16[1,8,2048]{2,1,0:T(8,128)(2,1)S(1)}, bf16[1,8,2048]{2,1,0:T(8,128)(2,1)}, u32[]{:S(2)}) copy-start(bf16[1,8,2048]{2,1,0:T(8,128)(2,1)} %param.15) | copy-start | bytes 98308
  7.9 0.7 %copy-start.7 = (f32[2048]{0:T(1024)S(1)}, f32[2048]{0:T(1024)}, u32[]{:S(2)}) copy-start(f32[2048]{0:T(1024)} %param.18) | copy-start | bytes 24580
  8.6 0.7 %copy-start.8 = (bf16[1,128]{1,0:T(2,128)(2,1)S(1)}, bf16[1,128]{1,0:T(2,128)(2,1)}, u32[]{:S(2)}) copy-start(bf16[1,128]{1,0:T(2,128)(2,1)} %condition.1) | copy-start | bytes 772
  9.3 0.7 %copy-start.9 = (bf16[128]{0:T(256)(128)(2,1)S(1)}, bf16[128]{0:T(256)(128)(2,1)}, u32[]{:S(2)}) copy-start(bf16[128]{0:T(256)(128)(2,1)} %param.16) | copy-start | bytes 772
  9.9 0.7 %copy-start.10 = (f32[128]{0:T(128)S(1)}, f32[128]{0:T(128)}, u32[]{:S(2)}) copy-start(f32[128]{0:T(128)} %param.22) | copy-start | bytes 1540
  10.6 0.7 %copy-start.11 = (f32[1,2]{1,0:T(1,128)S(1)}, f32[1,2]{1,0:T(1,128)}, u32[]{:S(2)}) copy-start(f32[1,2]{1,0:T(1,128)} %context_bias.1) | copy-start | bytes 28

commit v2 on v1

--- a/solution.py
+++ b/solution.py
@@ -192,13 +192,27 @@
 LANES = 128
 
 
+class Phases:
+    def __init__(self):
+        self.open = None
+
+    def __call__(self, name):
+        if self.open is not None:
+            self.open.__exit__(None, None, None)
+        self.open = None
+        if name is not None:
+            self.open = jax.named_scope(name)
+            self.open.__enter__()
+
+
 def fused_kernel(
     sp_n, tp_n, score_scale,
-    latent, condition, context, context_vector, modulator, norm_gain,
-    query_weight, key_weight, value_weight, head_gain, lambdas, context_bias, out_weight,
+    latent, condition_in, context, vector_in, modulator, gain_in,
+    query_weight, key_weight, value_weight, head_gain_in, lambdas_in, bias_in, out_weight,
     out,
+    condition, context_vector, norm_gain, head_gain, lambdas, context_bias,
     mod_v, part, rs_in, mods, lat, ctx_all, w_q, w_kv, w_out, vecs, hid, kvb, att_out, att_in,
-    own_sem, rs_ss, rs_rs, ag_ss, ag_rs, lat_ss, lat_rs, ctx_ss, ctx_rs,
+    small_sem, own_sem, rs_ss, rs_rs, ag_ss, ag_rs, lat_ss, lat_rs, ctx_ss, ctx_rs,
     kv_os, kv_ss, kv_rs, wt_ss, wt_rs, wd_ss, wd_rs, at_ss, at_rs,
 ):
     sp = lax.axis_index("sp")
@@ -212,6 +226,8 @@
     qrows = rows * tp_n
     chunk = part.shape[2]
 
+    phase = Phases()
+    phase("enter")
     barrier = pltpu.get_barrier_semaphore()
 
     def greet(d, carry):
@@ -224,6 +240,14 @@
     lax.fori_loop(1, n, greet, 0)
     pl.semaphore_signal(barrier, inc=1, device_id=(sp, tp, 1 - dp), device_id_type=MESH)
 
+    small = [
+        pltpu.make_async_copy(source, place, small_sem.at[k])
+        for k, (source, place) in enumerate((
+            (condition_in, condition), (vector_in, context_vector), (context, ctx_all.at[sp]),
+            (gain_in, norm_gain), (head_gain_in, head_gain), (lambdas_in, lambdas),
+            (bias_in, context_bias),
+        ))
+    ]
     loads = [
         pltpu.make_async_copy(modulator, mod_v, own_sem.at[0]),
         pltpu.make_async_copy(latent, lat.at[pl.ds(tp * 2, 2)], own_sem.at[1]),
@@ -232,9 +256,12 @@
         pltpu.make_async_copy(query_weight, w_q, own_sem.at[4]),
         pltpu.make_async_copy(out_weight, w_out.at[pl.ds(tp * 4, 4)], own_sem.at[5]),
     ]
-    for load in loads:
+    for load in small[:2] + loads[:2] + small[2:] + loads[2:]:
         load.start()
 
+    phase("partial")
+    for load in small:
+        load.wait()
     rows_in = jnp.concatenate([condition[...], context_vector[...]], axis=0).astype(jnp.float32)
     activated = jax.nn.silu(rows_in).astype(jnp.bfloat16)
     loads[0].wait()
@@ -242,7 +269,9 @@
     for p in range(n):
         part[p] = partial_terms[:, p * chunk : (p + 1) * chunk]
     loads[1].wait()
+    phase("barrier")
     pl.semaphore_wait(barrier, n)
+    phase("sends")
 
     def rs_copy(d):
         peer = lax.rem(rank + d, n)
@@ -313,22 +342,22 @@
     def ctx_copy(d):
         peer = lax.rem(sp + d, sp_n)
         return pltpu.make_async_remote_copy(
-            src_ref=context, dst_ref=ctx_all.at[sp], send_sem=ctx_ss.at[d], recv_sem=ctx_rs.at[d],
+            src_ref=ctx_all.at[sp], dst_ref=ctx_all.at[sp], send_sem=ctx_ss.at[d], recv_sem=ctx_rs.at[d],
             device_id=(peer, tp, dp), device_id_type=MESH,
         )
 
     def ctx_arrival(d):
         peer = lax.rem(sp - d + sp_n, sp_n)
         return pltpu.make_async_remote_copy(
-            src_ref=context, dst_ref=ctx_all.at[peer], send_sem=ctx_ss.at[d], recv_sem=ctx_rs.at[d],
+            src_ref=ctx_all.at[peer], dst_ref=ctx_all.at[peer], send_sem=ctx_ss.at[d], recv_sem=ctx_rs.at[d],
             device_id=(peer, tp, dp), device_id_type=MESH,
         )
 
     for d in range(1, sp_n):
         ctx_copy(d).start()
-    ctx_all[sp] = context[...]
     rs_in[0] = part[rank]
 
+    phase("rs_wait")
     each(1, n, lambda d: rs_copy(d).wait_recv())
     total = rs_in[0]
     for d in range(1, n):
@@ -336,16 +365,25 @@
     mods[rank] = total
     each(1, n, lambda d: ag_copy(d).start())
 
+    phase("lat_relay")
     lat_relays = plane.relays()
     plane.arrival(0, 0).wait_recv()
     lat_relays[0].start()
     plane.arrival(1, 1).wait_recv()
     lat_relays[1].start()
 
+    loads[5].wait()
+    wplane = Plane(w_out, lambda o, q: o * 4 + dp * 2 + q, wt_ss, wt_rs)
+    w_first = wplane.first()
+    for copy in w_first:
+        copy.start()
+
     for d in range(1, sp_n):
         ctx_arrival(d).wait_recv()
+    phase("ag_wait")
     each(1, n, lambda d: ag_arrival(d).wait_recv())
     whole = jnp.concatenate([mods[p] for p in range(n)], axis=1)
+    phase("vecs")
     gain = norm_gain[...]
     vecs[0:1, :] = gain * (1.0 + whole[0:1, width : 2 * width])
     vecs[1:2, :] = whole[0:1, :width]
@@ -368,6 +406,7 @@
         ctx_all[...].astype(jnp.float32).reshape(ctx_rows, width), 2
     )
     norm_block(tp)
+    phase("lat_rest")
     plane.arrival(0, 1).wait_recv()
     norm_block(across)
     plane.arrival(1, 0).wait_recv()
@@ -376,31 +415,27 @@
     plane.arrival(2, 1).wait_recv()
     norm_block(corner)
 
-    for load in loads[2:]:
+    phase("kv")
+    for load in loads[2:5]:
         load.wait()
     kv = jnp.dot(hid[...], w_kv[...], preferred_element_type=jnp.float32).astype(jnp.bfloat16)
-    kvb[sp] = kv[:qrows]
+    piece = qrows // 2
+    for q in range(2):
+        kvb[sp * 2 + q] = kv[q * piece : (q + 1) * piece]
     ctx_kv = kv[qrows:]
 
-    def kv_own(to, slot):
-        return pltpu.make_async_remote_copy(
-            src_ref=kvb.at[sp], dst_ref=kvb.at[sp], send_sem=kv_os.at[slot], recv_sem=kv_rs.at[sp],
-            device_id=(to, tp, dp), device_id_type=MESH,
-        )
-
-    @pl.when(sp + 1 < sp_n)
-    def _():
-        kv_own(sp + 1, 0).start()
-
-    @pl.when(sp > 0)
-    def _():
-        kv_own(sp - 1, 1).start()
-
-    wplane = Plane(w_out, lambda o, q: o * 4 + dp * 2 + q, wt_ss, wt_rs)
-    w_first = wplane.first()
-    for copy in w_first:
-        copy.start()
-
+    def kv_own(to, slot, q):
+        place = kvb.at[sp * 2 + q]
+        return pltpu.make_async_remote_copy(
+            src_ref=place, dst_ref=place, send_sem=kv_os.at[slot * 2 + q],
+            recv_sem=kv_rs.at[sp * 2 + q], device_id=(to, tp, dp), device_id_type=MESH,
+        )
+
+    for q in range(2):
+        pl.when(sp + 1 < sp_n)(lambda: kv_own(sp + 1, 0, q).start())
+        pl.when(sp > 0)(lambda: kv_own(sp - 1, 1, q).start())
+
+    phase("queries")
     queries = jnp.dot(hid[:qrows, :], w_q[...], preferred_element_type=jnp.float32) * score_scale
     queries = queries.astype(jnp.bfloat16)
     head = queries.shape[1] // 2
@@ -416,7 +451,7 @@
         )
 
     map_row = lax.broadcasted_iota(jnp.int32, (2 * qrows, 1), 0)
-    bias = jnp.where(map_row < qrows, context_bias[0, 0], context_bias[0, 1])
+    bias = jnp.where(map_row < qrows, context_bias[0:1, 0:1], context_bias[0:1, 1:2])
 
     def fold(running, scores, values):
         top = jnp.max(scores, axis=-1, keepdims=True)
@@ -431,14 +466,42 @@
             summed = running[2] * shrink + summed
         return top, count, summed
 
+    phase("fold_own")
     running = fold(None, score(ctx_kv[:, :LANES]) + bias, ctx_kv[:, LANES:])
     running = fold(running, score(kv[:qrows, :LANES]), kv[:qrows, LANES:])
 
+    def sibling(owner, part_no, slot):
+        place = w_out.at[owner * 4 + dp * 2 + part_no]
+        return pltpu.make_async_remote_copy(
+            src_ref=place, dst_ref=place, send_sem=wd_ss.at[slot], recv_sem=wd_rs.at[slot],
+            device_id=(sp, tp, 1 - dp), device_id_type=MESH,
+        )
+
+    def sibling_arrival(owner, part_no, slot):
+        place = w_out.at[owner * 4 + (1 - dp) * 2 + part_no]
+        return pltpu.make_async_remote_copy(
+            src_ref=place, dst_ref=place, send_sem=wd_ss.at[slot], recv_sem=wd_rs.at[slot],
+            device_id=(sp, tp, 1 - dp), device_id_type=MESH,
+        )
+
+    owners = (across, along, corner)
+    w_sent = []
+
+    def swap(kind, part_no, wait=True):
+        if wait:
+            wplane.arrival(kind, part_no).wait_recv()
+        copy = sibling(owners[kind], part_no, kind * 2 + part_no)
+        copy.start()
+        w_sent.append(copy)
+
+    phase("w_relay")
     w_relays = wplane.relays()
     wplane.arrival(0, 0).wait_recv()
     w_relays[0].start()
     wplane.arrival(1, 1).wait_recv()
     w_relays[1].start()
+    swap(0, 0, False)
+    swap(1, 1, False)
 
     high = (2 * sp) // sp_n
 
@@ -447,43 +510,38 @@
         down = (sp_n - t) - jnp.where(sp_n - t <= sp, 1, 0)
         return jnp.where(high == 0, up, down)
 
-    def onward(b):
+    def onward(b, q):
         step = jnp.where(b < sp, 1, -1)
         to = sp + step
         ok = jnp.logical_and(to >= 0, to < sp_n)
         safe = jnp.where(ok, to, sp - step)
         return ok, pltpu.make_async_remote_copy(
-            src_ref=kvb.at[b], dst_ref=kvb.at[b], send_sem=kv_ss.at[b], recv_sem=kv_rs.at[b],
-            device_id=(safe, tp, dp), device_id_type=MESH,
-        )
-
-    def sibling(owner, part_no, slot):
-        place = w_out.at[owner * 4 + dp * 2 + part_no]
-        return pltpu.make_async_remote_copy(
-            src_ref=place, dst_ref=place, send_sem=wd_ss.at[slot], recv_sem=wd_rs.at[slot],
-            device_id=(sp, tp, 1 - dp), device_id_type=MESH,
-        )
-
-    def sibling_arrival(owner, part_no, slot):
-        place = w_out.at[owner * 4 + (1 - dp) * 2 + part_no]
-        return pltpu.make_async_remote_copy(
-            src_ref=place, dst_ref=place, send_sem=wd_ss.at[slot], recv_sem=wd_rs.at[slot],
-            device_id=(sp, tp, 1 - dp), device_id_type=MESH,
-        )
-
-    owners = (across, along, corner)
+            src_ref=kvb.at[b * 2 + q], dst_ref=kvb.at[b * 2 + q], send_sem=kv_ss.at[b * 2 + q],
+            recv_sem=kv_rs.at[b * 2 + q], device_id=(safe, tp, dp), device_id_type=MESH,
+        )
+
     sent = []
-    for t in range(1, sp_n):
-        b = block_at(t)
-        ok, copy = onward(b)
-        copy.wait_recv()
-        pl.when(ok)(copy.start)
-        sent.append((ok, copy))
-        running = fold(running, score(kvb[b, :, :LANES]), kvb[b, :, LANES:])
-
+    for pair in range(1, sp_n, 2):
+        steps = [t for t in (pair, pair + 1) if t < sp_n]
+        phase(f"take{pair}")
+        for q in range(2):
+            for t in steps:
+                ok, copy = onward(block_at(t), q)
+                copy.wait_recv()
+                pl.when(ok)(copy.start)
+                sent.append((ok, copy))
+        phase(f"fold{pair}")
+        if pair == 1:
+            swap(0, 1)
+            swap(1, 0)
+        for t in steps:
+            block = kvb[pl.ds(block_at(t) * 2, 2)].reshape(qrows, 2 * LANES)
+            running = fold(running, score(block[:, :LANES]), block[:, LANES:])
+
+    phase("finish")
     top, count, summed = running
     shares = summed / count
-    mixed = shares[:qrows] - lambdas[0] * shares[qrows:]
+    mixed = shares[:qrows] - lambdas[...] * shares[qrows:]
     normed = (
         mixed
         * lax.rsqrt(jnp.mean(mixed * mixed, axis=-1, keepdims=True) + EPSILON)
@@ -511,19 +569,17 @@
         at_copy(d).start()
     att_in[tp] = att_out[tp]
 
-    w_sent = []
-    for kind, part_no in ((0, 0), (1, 1), (0, 1), (1, 0), (2, 0), (2, 1)):
-        if (kind, part_no) not in ((0, 0), (1, 1)):
-            wplane.arrival(kind, part_no).wait_recv()
-        copy = sibling(owners[kind], part_no, kind * 2 + part_no)
-        copy.start()
-        w_sent.append(copy)
+    phase("w_wait")
+    swap(2, 0)
+    swap(2, 1)
     for kind in range(3):
         for part_no in range(2):
             sibling_arrival(owners[kind], part_no, kind * 2 + part_no).wait_recv()
+    phase("at_wait")
     for d in range(1, tp_n):
         at_arrival(d).wait_recv()
 
+    phase("out")
     attended = jnp.concatenate([att_in[p] for p in range(tp_n)], axis=1)
     step = 512
     for first in range(0, width, step):
@@ -535,18 +591,21 @@
             update = mine + vecs[4:5, cols] * branch[q * half : (q + 1) * half]
             out[q * half : (q + 1) * half, cols] = update.astype(jnp.bfloat16)
 
+    phase("drain")
     each(1, n, lambda d: rs_copy(d).wait_send())
     each(1, n, lambda d: ag_copy(d).wait_send())
     for copy in lat_first + lat_relays + w_first + w_relays + w_sent:
         copy.wait_send()
     for d in range(1, sp_n):
         ctx_copy(d).wait_send()
-    pl.when(sp + 1 < sp_n)(lambda: kv_own(sp + 1, 0).wait_send())
-    pl.when(sp > 0)(lambda: kv_own(sp - 1, 1).wait_send())
+    for q in range(2):
+        pl.when(sp + 1 < sp_n)(lambda: kv_own(sp + 1, 0, q).wait_send())
+        pl.when(sp > 0)(lambda: kv_own(sp - 1, 1, q).wait_send())
     for ok, copy in sent:
         pl.when(ok)(copy.wait_send)
     for d in range(1, tp_n):
         at_copy(d).wait_send()
+    phase(None)
 
 
 def fused(
@@ -565,15 +624,20 @@
     wrows = out_weight.shape[0] // 4
     bf, f32 = jnp.bfloat16, jnp.float32
     vm = pl.BlockSpec(memory_space=pltpu.VMEM)
-    sm = pl.BlockSpec(memory_space=pltpu.SMEM)
-    hb = pl.BlockSpec(memory_space=pl.ANY)
+    hb = pl.BlockSpec(memory_space=pltpu.HBM)
     dma = lambda k: pltpu.SemaphoreType.DMA((k,))
     result = pl.pallas_call(
         functools.partial(fused_kernel, sp_n, tp_n, (qw // 2) ** (-0.5)),
-        out_shape=jax.ShapeDtypeStruct((rows, width), bf),
-        in_specs=[hb, vm, vm, vm, hb, vm, hb, hb, hb, vm, sm, sm, hb],
+        out_shape=pltpu.VMEM((rows, width), bf),
+        in_specs=[hb] * 13,
         out_specs=vm,
         scratch_shapes=[
+            pltpu.VMEM(condition.shape, bf),
+            pltpu.VMEM((1, context_vector.shape[0]), bf),
+            pltpu.VMEM((1, width), f32),
+            pltpu.VMEM((1, value), f32),
+            pltpu.VMEM((1, 1), f32),
+            pltpu.VMEM(context_bias.shape, f32),
             pltpu.VMEM(modulator.shape, bf),
             pltpu.VMEM((n, 2, chunk), f32),
             pltpu.VMEM((n, 2, chunk), f32),
@@ -585,14 +649,14 @@
             pltpu.VMEM((tp_n * 4, wrows, width), bf),
             pltpu.VMEM((8, width), f32),
             pltpu.VMEM((qrows + sp_n * ctx_rows, width), bf),
-            pltpu.VMEM((sp_n, qrows, qw + value), bf),
+            pltpu.VMEM((sp_n * 2, qrows // 2, qw + value), bf),
             pltpu.VMEM((tp_n, rows, value), bf),
             pltpu.VMEM((tp_n, rows, value), bf),
-            dma(6), dma(n), dma(n), dma(n), dma(n), dma(6), dma(6), dma(sp_n), dma(sp_n),
-            dma(2), dma(sp_n), dma(sp_n), dma(6), dma(6), dma(6), dma(6), dma(tp_n), dma(tp_n),
+            dma(7), dma(6), dma(n), dma(n), dma(n), dma(n), dma(6), dma(6), dma(sp_n), dma(sp_n),
+            dma(4), dma(sp_n * 2), dma(sp_n * 2), dma(6), dma(6), dma(6), dma(6), dma(tp_n), dma(tp_n),
         ],
         compiler_params=pltpu.CompilerParams(
-            collective_id=0, has_side_effects=True, vmem_limit_bytes=48 * 2**20
+            collective_id=0, has_side_effects=True, vmem_limit_bytes=66700000
         ),
         name="fused_block",
     )(
@@ -606,7 +670,7 @@
         key_weight,
         value_weight,
         head_gain[None, :],
-        lambdas,
+        lambdas[None, :],
         context_bias,
         out_weight.reshape(4, wrows, width),
     )

time: 50 us -> 37.1 us (0.74)
  local copies, waits for them, and re-layouts: 11.3 us -> 0.71 us
  Pallas kernels: 37.5 us -> 35.6 us
    unnamed x25 -> x1, local copies, waits for them, and re-layouts: 11.3 us -> 0.71 us
    pallas_call x1, Pallas kernels: 37.5 us -> 35.6 us  [fused(): pl.pallas_call(functools.partial(fused_kernel, sp_n, tp_n, (qw // 2) ** (...]
where the time goes in v2:
time: 37.1 us; the launch traced here: 37 us
  Pallas kernels  35.6 us (96%)
  local copies, waits for them, and re-layouts  0.71 us (2%)
  between operations  0.66 us (2%)
    pallas_call x1, Pallas kernels, fused(): pl.pallas_call(functools.partial(fused_kernel, sp_n, tp_n, (qw // 2) ** (...  35.6 us

profile of v2, /device:TPU:0, one launch (start us, length us, event | category | flops | bytes accessed | tf_op | source)
XLA Modules:
  0.0 37.0 jit_solution(13365108524085040598)
XLA Ops:
  0.7 35.6 %fused_block.1 = bf16[64,2048]{1,0:T(8,128)(2,1)S(1)} custom-call(bf16[2,32,2048]{2,1,0:T(8,128)(2,1)} %bitcast.11, bf16[1,128]{1,0:T(2,128)(2,1)} %condition_in.1, bf16[8,2048]{1,0:T(8,128)(2,1)} %bitcast.12, bf16[1,128]{1,0:T(2,128)(2,1)} %bitcast.14, bf16[128,6144]{1,0:T(8,128)(2,1)} %modulator.1, f32[1,2048]{1,0:T(1,128)} %bitcast.13, ...), custom_call_target="tpu_custom_call" | custom-call | tf_op jit(solution)/shard_map/fused_block/pallas_call | solution.py:629
  36.2 0.7 %copy.15 = bf16[1,64,2048]{2,1,0:T(8,128)(2,1)} copy(bf16[1,64,2048]{2,1,0:T(8,128)(2,1)S(1)} %bitcast.9) | data formatting | bytes 524288

commit v3 on v2

--- a/solution.py
+++ b/solution.py
@@ -220,6 +220,10 @@
     dp = lax.axis_index("dp")
     n = sp_n * tp_n
     rank = sp * tp_n + tp
+    across = tp + 1 - 2 * lax.rem(tp, 2)
+    along = lax.rem(tp + 2, 4)
+    corner = along + 1 - 2 * lax.rem(along, 2)
+    roles = (tp, across, along, corner)
     half = lat.shape[1]
     width = lat.shape[2]
     rows = half * 2
@@ -229,16 +233,6 @@
     phase = Phases()
     phase("enter")
     barrier = pltpu.get_barrier_semaphore()
-
-    def greet(d, carry):
-        peer = lax.rem(rank + d, n)
-        pl.semaphore_signal(
-            barrier, inc=1, device_id=(peer // tp_n, lax.rem(peer, tp_n), dp), device_id_type=MESH
-        )
-        return carry
-
-    lax.fori_loop(1, n, greet, 0)
-    pl.semaphore_signal(barrier, inc=1, device_id=(sp, tp, 1 - dp), device_id_type=MESH)
 
     small = [
         pltpu.make_async_copy(source, place, small_sem.at[k])
@@ -259,6 +253,16 @@
     for load in small[:2] + loads[:2] + small[2:] + loads[2:]:
         load.start()
 
+    def greet(d, carry):
+        peer = lax.rem(rank + d, n)
+        pl.semaphore_signal(
+            barrier, inc=1, device_id=(peer // tp_n, lax.rem(peer, tp_n), dp), device_id_type=MESH
+        )
+        return carry
+
+    lax.fori_loop(1, n, greet, 0)
+    pl.semaphore_signal(barrier, inc=1, device_id=(sp, tp, 1 - dp), device_id_type=MESH)
+
     phase("partial")
     for load in small:
         load.wait()
@@ -276,22 +280,29 @@
     def rs_copy(d):
         peer = lax.rem(rank + d, n)
         return pltpu.make_async_remote_copy(
-            src_ref=part.at[peer], dst_ref=rs_in.at[d], send_sem=rs_ss.at[d], recv_sem=rs_rs.at[d],
+            src_ref=part.at[peer], dst_ref=rs_in.at[d], send_sem=rs_ss.at[0], recv_sem=rs_rs.at[0],
             device_id=(peer // tp_n, lax.rem(peer, tp_n), dp), device_id_type=MESH,
         )
 
     def ag_copy(d):
         peer = lax.rem(rank + d, n)
         return pltpu.make_async_remote_copy(
-            src_ref=mods.at[rank], dst_ref=mods.at[rank], send_sem=ag_ss.at[d], recv_sem=ag_rs.at[d],
+            src_ref=mods.at[rank], dst_ref=mods.at[rank], send_sem=ag_ss.at[0], recv_sem=ag_rs.at[0],
             device_id=(peer // tp_n, lax.rem(peer, tp_n), dp), device_id_type=MESH,
         )
 
-    def ag_arrival(d):
-        peer = lax.rem(rank - d + n, n)
-        return pltpu.make_async_remote_copy(
-            src_ref=mods.at[peer], dst_ref=mods.at[peer], send_sem=ag_ss.at[d], recv_sem=ag_rs.at[d],
-            device_id=(peer // tp_n, lax.rem(peer, tp_n), dp), device_id_type=MESH,
+    def rs_all():
+        return pltpu.make_async_remote_copy(
+            src_ref=part.at[pl.ds(0, n - 1)], dst_ref=rs_in.at[pl.ds(1, n - 1)],
+            send_sem=rs_ss.at[0], recv_sem=rs_rs.at[0],
+            device_id=(sp, across, dp), device_id_type=MESH,
+        )
+
+    def ag_all():
+        return pltpu.make_async_remote_copy(
+            src_ref=mods.at[pl.ds(0, n - 1)], dst_ref=mods.at[pl.ds(0, n - 1)],
+            send_sem=ag_ss.at[0], recv_sem=ag_rs.at[0],
+            device_id=(sp, across, dp), device_id_type=MESH,
         )
 
     def each(first, last, act):
@@ -303,9 +314,6 @@
 
     each(1, n, lambda d: rs_copy(d).start())
 
-    across = tp + 1 - 2 * lax.rem(tp, 2)
-    along = lax.rem(tp + 2, 4)
-    corner = along + 1 - 2 * lax.rem(along, 2)
 
     class Plane:
         def __init__(self, buf, index, ss, rs):
@@ -358,7 +366,7 @@
     rs_in[0] = part[rank]
 
     phase("rs_wait")
-    each(1, n, lambda d: rs_copy(d).wait_recv())
+    rs_all().wait_recv()
     total = rs_in[0]
     for d in range(1, n):
         total = total + rs_in[d]
@@ -381,7 +389,7 @@
     for d in range(1, sp_n):
         ctx_arrival(d).wait_recv()
     phase("ag_wait")
-    each(1, n, lambda d: ag_arrival(d).wait_recv())
+    ag_all().wait_recv()
     whole = jnp.concatenate([mods[p] for p in range(n)], axis=1)
     phase("vecs")
     gain = norm_gain[...]
@@ -396,44 +404,52 @@
         scale = lax.rsqrt(jnp.mean(x * x, axis=-1, keepdims=True) + EPSILON)
         return (x * scale * vecs[at : at + 1, :] + vecs[at + 1 : at + 2, :]).astype(jnp.bfloat16)
 
-    def norm_block(owner):
+    def norm_block(role):
         for q in range(2):
-            at = pl.multiple_of((owner * 2 + q) * half, half)
-            hid[pl.ds(at, half), :] = normed_rows(lat[owner * 2 + q], 0)
-
+            at = (role * 2 + q) * half
+            hid[at : at + half, :] = normed_rows(lat[roles[role] * 2 + q], 0)
+
+    def kv_own(to, slot, q):
+        place = kvb.at[sp * 2 + q]
+        return pltpu.make_async_remote_copy(
+            src_ref=place, dst_ref=place, send_sem=kv_os.at[slot * 2 + q],
+            recv_sem=kv_rs.at[sp * 2 + q], device_id=(to, tp, dp), device_id_type=MESH,
+        )
+
+    def kv_rows(first, last):
+        product = jnp.dot(hid[first:last, :], w_kv[...], preferred_element_type=jnp.float32)
+        return product.astype(jnp.bfloat16)
+
+    def kv_send(q):
+        pl.when(sp + 1 < sp_n)(lambda: kv_own(sp + 1, 0, q).start())
+        pl.when(sp > 0)(lambda: kv_own(sp - 1, 1, q).start())
+
+    piece = qrows // 2
     ctx_rows = ctx_all.shape[0] * ctx_all.shape[1]
+    norm_block(0)
+    plane.arrival(0, 1).wait_recv()
+    norm_block(1)
+    phase("kv0")
+    for load in loads[2:5]:
+        load.wait()
+    kv_near = kv_rows(0, piece)
+    kvb[sp * 2] = kv_near
+    kv_send(0)
+    phase("lat_rest")
     hid[qrows : qrows + ctx_rows, :] = normed_rows(
         ctx_all[...].astype(jnp.float32).reshape(ctx_rows, width), 2
     )
-    norm_block(tp)
-    phase("lat_rest")
-    plane.arrival(0, 1).wait_recv()
-    norm_block(across)
     plane.arrival(1, 0).wait_recv()
-    norm_block(along)
+    norm_block(2)
     plane.arrival(2, 0).wait_recv()
     plane.arrival(2, 1).wait_recv()
-    norm_block(corner)
-
-    phase("kv")
-    for load in loads[2:5]:
-        load.wait()
-    kv = jnp.dot(hid[...], w_kv[...], preferred_element_type=jnp.float32).astype(jnp.bfloat16)
-    piece = qrows // 2
-    for q in range(2):
-        kvb[sp * 2 + q] = kv[q * piece : (q + 1) * piece]
-    ctx_kv = kv[qrows:]
-
-    def kv_own(to, slot, q):
-        place = kvb.at[sp * 2 + q]
-        return pltpu.make_async_remote_copy(
-            src_ref=place, dst_ref=place, send_sem=kv_os.at[slot * 2 + q],
-            recv_sem=kv_rs.at[sp * 2 + q], device_id=(to, tp, dp), device_id_type=MESH,
-        )
-
-    for q in range(2):
-        pl.when(sp + 1 < sp_n)(lambda: kv_own(sp + 1, 0, q).start())
-        pl.when(sp > 0)(lambda: kv_own(sp - 1, 1, q).start())
+    norm_block(3)
+    phase("kv1")
+    kv_far = kv_rows(piece, qrows + ctx_rows)
+    kvb[sp * 2 + 1] = kv_far[:piece]
+    kv_send(1)
+    kv = jnp.concatenate([kv_near, kv_far[:piece]], axis=0)
+    ctx_kv = kv_far[piece:]
 
     phase("queries")
     queries = jnp.dot(hid[:qrows, :], w_q[...], preferred_element_type=jnp.float32) * score_scale
@@ -468,7 +484,7 @@
 
     phase("fold_own")
     running = fold(None, score(ctx_kv[:, :LANES]) + bias, ctx_kv[:, LANES:])
-    running = fold(running, score(kv[:qrows, :LANES]), kv[:qrows, LANES:])
+    running = fold(running, score(kv[:, :LANES]), kv[:, LANES:])
 
     def sibling(owner, part_no, slot):
         place = w_out.at[owner * 4 + dp * 2 + part_no]
@@ -552,22 +568,20 @@
         att_out[p] = normed[p * rows : (p + 1) * rows]
 
     def at_copy(d):
-        peer = lax.rem(tp + d, tp_n)
-        return pltpu.make_async_remote_copy(
-            src_ref=att_out.at[peer], dst_ref=att_in.at[tp], send_sem=at_ss.at[d], recv_sem=at_rs.at[d],
-            device_id=(sp, peer, dp), device_id_type=MESH,
+        return pltpu.make_async_remote_copy(
+            src_ref=att_out.at[d], dst_ref=att_in.at[tp], send_sem=at_ss.at[d], recv_sem=at_rs.at[d],
+            device_id=(sp, roles[d], dp), device_id_type=MESH,
         )
 
     def at_arrival(d):
-        peer = lax.rem(tp - d + tp_n, tp_n)
-        return pltpu.make_async_remote_copy(
-            src_ref=att_out.at[peer], dst_ref=att_in.at[peer], send_sem=at_ss.at[d], recv_sem=at_rs.at[d],
-            device_id=(sp, peer, dp), device_id_type=MESH,
-        )
-
-    for d in range(1, tp_n):
+        return pltpu.make_async_remote_copy(
+            src_ref=att_out.at[d], dst_ref=att_in.at[roles[d]], send_sem=at_ss.at[d],
+            recv_sem=at_rs.at[d], device_id=(sp, roles[d], dp), device_id_type=MESH,
+        )
+
+    for d in (3, 1, 2):
         at_copy(d).start()
-    att_in[tp] = att_out[tp]
+    att_in[tp] = att_out[0]
 
     phase("w_wait")
     swap(2, 0)
@@ -592,8 +606,8 @@
             out[q * half : (q + 1) * half, cols] = update.astype(jnp.bfloat16)
 
     phase("drain")
-    each(1, n, lambda d: rs_copy(d).wait_send())
-    each(1, n, lambda d: ag_copy(d).wait_send())
+    rs_all().wait_send()
+    ag_all().wait_send()
     for copy in lat_first + lat_relays + w_first + w_relays + w_sent:
         copy.wait_send()
     for d in range(1, sp_n):
@@ -652,7 +666,7 @@
             pltpu.VMEM((sp_n * 2, qrows // 2, qw + value), bf),
             pltpu.VMEM((tp_n, rows, value), bf),
             pltpu.VMEM((tp_n, rows, value), bf),
-            dma(7), dma(6), dma(n), dma(n), dma(n), dma(n), dma(6), dma(6), dma(sp_n), dma(sp_n),
+            dma(7), dma(6), dma(1), dma(1), dma(1), dma(1), dma(6), dma(6), dma(sp_n), dma(sp_n),
             dma(4), dma(sp_n * 2), dma(sp_n * 2), dma(6), dma(6), dma(6), dma(6), dma(tp_n), dma(tp_n),
         ],
         compiler_params=pltpu.CompilerParams(

time: 37.1 us -> 35.1 us (0.946)
  Pallas kernels: 35.6 us -> 33.5 us
    pallas_call x1, Pallas kernels: 35.6 us -> 33.5 us  [fused(): pl.pallas_call(functools.partial(fused_kernel, sp_n, tp_n, (qw // 2) ** (...]
where the time goes in v3:
time: 35.1 us; the launch traced here: 34.9 us
  Pallas kernels  33.5 us (95%)
  local copies, waits for them, and re-layouts  0.71 us (2%)
  between operations  0.66 us (2%)
    pallas_call x1, Pallas kernels, fused(): pl.pallas_call(functools.partial(fused_kernel, sp_n, tp_n, (qw // 2) ** (...  33.5 us
    unnamed x1, local copies, waits for them, and re-layouts  0.71 us

profile of v3, /device:TPU:0, one launch (start us, length us, event | category | flops | bytes accessed | tf_op | source)
XLA Modules:
  0.0 34.9 jit_solution(1204104822509194131)
XLA Ops:
  0.7 33.5 %fused_block.1 = bf16[64,2048]{1,0:T(8,128)(2,1)S(1)} custom-call(bf16[2,32,2048]{2,1,0:T(8,128)(2,1)} %bitcast.11, bf16[1,128]{1,0:T(2,128)(2,1)} %condition_in.1, bf16[8,2048]{1,0:T(8,128)(2,1)} %bitcast.12, bf16[1,128]{1,0:T(2,128)(2,1)} %bitcast.14, bf16[128,6144]{1,0:T(8,128)(2,1)} %modulator.1, f32[1,2048]{1,0:T(1,128)} %bitcast.13, ...), custom_call_target="tpu_custom_call" | custom-call | tf_op jit(solution)/shard_map/fused_block/pallas_call | solution.py:643
  34.2 0.7 %copy.15 = bf16[1,64,2048]{2,1,0:T(8,128)(2,1)} copy(bf16[1,64,2048]{2,1,0:T(8,128)(2,1)S(1)} %bitcast.9) | data formatting | bytes 524288

commit v4 on v3

--- a/solution.py
+++ b/solution.py
@@ -510,6 +510,34 @@
         copy.start()
         w_sent.append(copy)
 
+    high = (2 * sp) // sp_n
+
+    def block_at(t):
+        up = (t - 1) + jnp.where(t - 1 >= sp, 1, 0)
+        down = (sp_n - t) - jnp.where(sp_n - t <= sp, 1, 0)
+        return jnp.where(high == 0, up, down)
+
+    def onward(b, q):
+        step = jnp.where(b < sp, 1, -1)
+        to = sp + step
+        ok = jnp.logical_and(to >= 0, to < sp_n)
+        safe = jnp.where(ok, to, sp - step)
+        return ok, pltpu.make_async_remote_copy(
+            src_ref=kvb.at[b * 2 + q], dst_ref=kvb.at[b * 2 + q], send_sem=kv_ss.at[b * 2 + q],
+            recv_sem=kv_rs.at[b * 2 + q], device_id=(safe, tp, dp), device_id_type=MESH,
+        )
+
+    sent = []
+    def take(t, q):
+        ok, copy = onward(block_at(t), q)
+        copy.wait_recv()
+        pl.when(ok)(copy.start)
+        sent.append((ok, copy))
+
+    near = [t for t in (1, 2) if t < sp_n]
+    phase("take_near")
+    for t in near:
+        take(t, 0)
     phase("w_relay")
     w_relays = wplane.relays()
     wplane.arrival(0, 0).wait_recv()
@@ -519,39 +547,20 @@
     swap(0, 0, False)
     swap(1, 1, False)
 
-    high = (2 * sp) // sp_n
-
-    def block_at(t):
-        up = (t - 1) + jnp.where(t - 1 >= sp, 1, 0)
-        down = (sp_n - t) - jnp.where(sp_n - t <= sp, 1, 0)
-        return jnp.where(high == 0, up, down)
-
-    def onward(b, q):
-        step = jnp.where(b < sp, 1, -1)
-        to = sp + step
-        ok = jnp.logical_and(to >= 0, to < sp_n)
-        safe = jnp.where(ok, to, sp - step)
-        return ok, pltpu.make_async_remote_copy(
-            src_ref=kvb.at[b * 2 + q], dst_ref=kvb.at[b * 2 + q], send_sem=kv_ss.at[b * 2 + q],
-            recv_sem=kv_rs.at[b * 2 + q], device_id=(safe, tp, dp), device_id_type=MESH,
-        )
-
-    sent = []
-    for pair in range(1, sp_n, 2):
-        steps = [t for t in (pair, pair + 1) if t < sp_n]
-        phase(f"take{pair}")
+    phase("take_near2")
+    for t in near:
+        take(t, 1)
+    swap(0, 1)
+    swap(1, 0)
+    phase("fold_near")
+    for t in near:
+        block = kvb[pl.ds(block_at(t) * 2, 2)].reshape(qrows, 2 * LANES)
+        running = fold(running, score(block[:, :LANES]), block[:, LANES:])
+    for t in range(3, sp_n):
         for q in range(2):
-            for t in steps:
-                ok, copy = onward(block_at(t), q)
-                copy.wait_recv()
-                pl.when(ok)(copy.start)
-                sent.append((ok, copy))
-        phase(f"fold{pair}")
-        if pair == 1:
-            swap(0, 1)
-            swap(1, 0)
-        for t in steps:
-            block = kvb[pl.ds(block_at(t) * 2, 2)].reshape(qrows, 2 * LANES)
+            phase(f"take{t}_{q}")
+            take(t, q)
+            block = kvb[block_at(t) * 2 + q]
             running = fold(running, score(block[:, :LANES]), block[:, LANES:])
 
     phase("finish")

time: 35.1 us -> 35 us (level)
  no operation moved by 1% of the time
where the time goes in v4:
time: 35 us; the launch traced here: 34.8 us
  Pallas kernels  33.5 us (96%)
  local copies, waits for them, and re-layouts  0.71 us (2%)
  between operations  0.66 us (2%)
    pallas_call x1, Pallas kernels, fused(): pl.pallas_call(functools.partial(fused_kernel, sp_n, tp_n, (qw // 2) ** (...  33.5 us
    unnamed x1, local copies, waits for them, and re-layouts  0.71 us

profile of v4, /device:TPU:0, one launch (start us, length us, event | category | flops | bytes accessed | tf_op | source)
XLA Modules:
  0.0 34.8 jit_solution(13135175720160012185)
XLA Ops:
  0.7 33.5 %fused_block.1 = bf16[64,2048]{1,0:T(8,128)(2,1)S(1)} custom-call(bf16[2,32,2048]{2,1,0:T(8,128)(2,1)} %bitcast.11, bf16[1,128]{1,0:T(2,128)(2,1)} %condition_in.1, bf16[8,2048]{1,0:T(8,128)(2,1)} %bitcast.12, bf16[1,128]{1,0:T(2,128)(2,1)} %bitcast.14, bf16[128,6144]{1,0:T(8,128)(2,1)} %modulator.1, f32[1,2048]{1,0:T(1,128)} %bitcast.13, ...), custom_call_target="tpu_custom_call" | custom-call | tf_op jit(solution)/shard_map/fused_block/pallas_call | solution.py:652
  34.1 0.7 %copy.15 = bf16[1,64,2048]{2,1,0:T(8,128)(2,1)} copy(bf16[1,64,2048]{2,1,0:T(8,128)(2,1)S(1)} %bitcast.9) | data formatting | bytes 524288
